TPU v7x, 512 devices: a 4x2x32 block of a 4x8x32 slice. The times are simulated.
512 devices in a mesh: grp: 2 (over y), sp: 32 (over z), tp: 8 (over x, core).
Axes of the slice: x: 4, y: 2, z: 32, core: 2. Of those that a mesh axis runs over, the one named last changes fastest.
The devices are a block of a 4x8x32 slice.
Arguments:
- starting_stream: bfloat16 [24576, 2048], P(('grp', 'sp'), 'tp'), parts along dimension 0, may hold values from -45 to 45
- multiplier_matrix: bfloat16 [2, 2048, 2048], P(None, 'sp', 'tp'), may hold values from -0.125 to 0.125
- memory_path_matrix: bfloat16 [2, 2048, 2048], P(None, 'sp', 'tp'), may hold values from -0.125 to 0.125
- filter_coefficients: bfloat16 [2, 4, 2048], P(None, None, 'tp'), may hold values from -3 to 3
- memory_valve_matrix: bfloat16 [2, 8, 256, 256], P(None, 'tp'), may hold values from -0.375 to 0.375
- entry_valve_matrix: bfloat16 [2, 8, 256, 256], P(None, 'tp'), may hold values from -0.375 to 0.375
- forgetting_parameters: float32 [2, 2048], P(None, 'tp'), may hold values from 3 to 15
- timestep_forgetting_multiplier: float32 [24576], P(('grp', 'sp')), parts along dimension 0, may hold values from 0.5 to 2
- spike_extra: float32 [24576, 2048], P(('grp', 'sp'), 'tp'), parts along dimension 0, may hold values from -0.7 to 0
- exit_projector_matrix: bfloat16 [2, 2048, 2048], P(None, 'tp', 'sp'), may hold values from -0.125 to 0.125
- prelude_rms_gains: float32 [2, 2048], replicated, may hold values from 0.1 to 1.9
- finishing_rms_gains: float32 [2048], P('tp'), may hold values from 0.1 to 1.9
Outputs:
- result: bfloat16 [24576, 2048], P(('grp', 'sp'), 'tp'), parts along dimension 0
There are 2 independent parts, one for each index of `grp`. A program takes and returns all parts, laid end to end along the dimension named above; an argument that names none is the same for every part. Nothing has to cross between parts.
All inputs are finite; a program needn't handle non-finite values.
Results may differ from a plain program's by a relative error of at most 0.015.
Values may be sent and summed in bfloat16 or wider, within the bound.
A program may use at most 64 MiB of HBM per device.

v0:
```python
import jax
import jax.numpy as jnp
from jax import lax
from jax.sharding import PartitionSpec as P

BLOCK_W = 256
EPSILON = 1e-06
SQUASH_POWER = 8.0


def sent_to_all(x, axis):
    copies = jnp.broadcast_to(x, (lax.axis_size(axis), *x.shape))
    return lax.all_to_all(copies, axis, split_axis=0, concat_axis=0, tiled=True)


def laid_out(tiles, dim):
    lengths = list(tiles.shape[1:])
    lengths[dim] *= tiles.shape[0]
    return jnp.moveaxis(tiles, 0, dim).reshape(lengths)


def gather_directly(x, axis, dim):
    tiles = sent_to_all(x, axis)
    return laid_out(tiles, dim)


def in_one_piece(arrays, axis, dim, along):
    widths = [a.shape[along] for a in arrays]
    both = jnp.concatenate(arrays, axis=along)
    whole = lax.all_gather(both, axis, axis=dim, tiled=True)
    return tuple(jnp.split(whole, [sum(widths[:k]) for k in range(1, len(widths))], axis=along))


def from_behind(value, axis, steps):
    count = lax.axis_size(axis)
    first, last = (max(0, -steps), min(count, count - steps))
    return lax.ppermute(value, axis, [(source, source + steps) for source in range(first, last)])


def gathered_once(x, axis):
    leaves = jax.tree.leaves(x)
    turns = sorted(range(len(leaves)), key=lambda k: -leaves[k].size)
    width = (1, *leaves[turns[0]].shape)[-1]
    lines = [
        jnp.pad(leaves[k].reshape(-1), (0, -leaves[k].size % width)).reshape(-1, width)
        for k in turns
    ]
    both, at, found = (lax.all_gather(jnp.concatenate(lines), axis), 0, {})
    for k, line in zip(turns, lines):
        slab = both[:, at : at + len(line)].reshape(len(both), -1)
        found[k] = slab[:, : leaves[k].size].reshape(-1, *leaves[k].shape)
        at += len(line)
    numbers = iter(range(len(leaves)))
    return jax.tree.map(lambda _: found[next(numbers)], x)


def carried_in(part, axis, combine, identity):
    place = lax.axis_index(axis)
    gathered = gathered_once(part, axis)
    state = jax.tree.map(lambda a, e: jnp.zeros_like(a) + jnp.asarray(e, a.dtype), part, identity)

    def one(lap, state):
        return combine(
            state, jax.tree.map(lambda a: lax.dynamic_index_in_dim(a, lap, 0, False), gathered)
        )

    return lax.fori_loop(0, place, one, state)


def split_up(x, dim, count):
    before, after = (x.shape[:dim], x.shape[dim + 1 :])
    return jnp.moveaxis(x.reshape(*before, count, -1, *after), dim, 0)


def summed_on_arrival(x, axis, dim):
    tiles = split_up(x, dim, lax.axis_size(axis))
    arrived = lax.all_to_all(tiles, axis, split_axis=0, concat_axis=0, tiled=True)
    return arrived.astype(jnp.float32).sum(axis=0)


def of_everyone(x, axis):
    everything = sent_to_all(x, axis)
    return jnp.sum(everything, axis=0)


def combine_pairs(earlier, later):
    return (earlier[0] * later[0], later[0] * earlier[1] + later[1])


def gather_rows(own_cols):
    return gather_directly(own_cols, "tp", 1)


def fetch_layer(multiplier_matrix, memory_path_matrix, exit_projector_matrix, tier_number):
    in_pair = in_one_piece(
        (multiplier_matrix[tier_number], memory_path_matrix[tier_number]), "sp", 0, 1
    )
    out_full = lax.all_gather(exit_projector_matrix[tier_number], "sp", axis=1, tiled=True)
    return (in_pair[0], in_pair[1], out_full)


def on_device(
    starting_stream,
    multiplier_matrix,
    memory_path_matrix,
    filter_coefficients,
    memory_valve_matrix,
    entry_valve_matrix,
    forgetting_parameters,
    timestep_forgetting_multiplier,
    spike_extra,
    exit_projector_matrix,
    prelude_rms_gains,
    finishing_rms_gains,
):
    tok_rows = starting_stream.shape[0]
    channels = memory_path_matrix.shape[2]
    own_cols = starting_stream
    full_rows = gather_rows(starting_stream)
    fetched = fetch_layer(multiplier_matrix, memory_path_matrix, exit_projector_matrix, 0)
    for tier_number in range(memory_path_matrix.shape[0]):
        floats = full_rows.astype(jnp.float32)
        mean_square = jnp.mean(floats * floats, axis=1, keepdims=True)
        normed = (
            floats * lax.rsqrt(mean_square + EPSILON) * prelude_rms_gains[tier_number][None, :]
        ).astype(jnp.bfloat16)
        branch_acc = jnp.dot(normed, fetched[0], preferred_element_type=jnp.float32)
        recur_acc = jnp.dot(normed, fetched[1], preferred_element_type=jnp.float32)
        out_full = fetched[2]
        if tier_number + 1 < memory_path_matrix.shape[0]:
            fetched = fetch_layer(
                multiplier_matrix, memory_path_matrix, exit_projector_matrix, tier_number + 1
            )
        branch = branch_acc.astype(jnp.bfloat16)
        recurrent = recur_acc.astype(jnp.bfloat16)
        taps_now = filter_coefficients[tier_number]
        reach_back = taps_now.shape[0] - 1
        halo_rows = from_behind(recurrent[tok_rows - reach_back :], "sp", 1)
        extended = jnp.concatenate([halo_rows, recurrent], axis=0)
        conv_sum = jnp.zeros((tok_rows, channels), jnp.float32)
        for offset in range(taps_now.shape[0]):
            conv_sum = conv_sum + extended[offset : offset + tok_rows].astype(
                jnp.float32
            ) * taps_now[offset].astype(jnp.float32)
        convolved = conv_sum.astype(jnp.bfloat16)
        blocks = convolved.reshape(tok_rows, channels // BLOCK_W, BLOCK_W)
        reset_gate = jax.nn.sigmoid(
            jnp.einsum(
                "tnc,ncd->tnd",
                blocks,
                memory_valve_matrix[tier_number],
                preferred_element_type=jnp.float32,
            ).reshape(tok_rows, channels)
        )
        inject = jax.nn.sigmoid(
            jnp.einsum(
                "tnc,ncd->tnd",
                blocks,
                entry_valve_matrix[tier_number],
                preferred_element_type=jnp.float32,
            ).reshape(tok_rows, channels)
        )
        logarithmic_persistence = (
            -SQUASH_POWER
            * reset_gate
            * jax.nn.softplus(-forgetting_parameters[tier_number])[None, :]
            * timestep_forgetting_multiplier[:, None]
            + spike_extra
        )
        keep_rate = jnp.exp(logarithmic_persistence)
        driven = (
            inject
            * convolved.astype(jnp.float32)
            * jnp.sqrt(-jnp.expm1(2.0 * logarithmic_persistence))
        )
        keep_cum, state_local = lax.associative_scan(combine_pairs, (keep_rate, driven), axis=0)
        identity = (jnp.ones((channels,), jnp.float32), jnp.zeros((channels,), jnp.float32))
        carried = carried_in((keep_cum[-1], state_local[-1]), "sp", combine_pairs, identity)
        state_seq = state_local + keep_cum * carried[1][None, :]
        mixed_in = (jax.nn.gelu(branch.astype(jnp.float32)) * state_seq).astype(jnp.bfloat16)
        partial_value = jnp.dot(mixed_in, out_full, preferred_element_type=jnp.float32)
        mixed_sum = summed_on_arrival(partial_value.astype(jnp.bfloat16), "tp", 1)
        own_cols = (own_cols.astype(jnp.float32) + mixed_sum).astype(jnp.bfloat16)
        if tier_number + 1 < memory_path_matrix.shape[0]:
            full_rows = gather_rows(own_cols)
    floats = own_cols.astype(jnp.float32)
    full_width = floats.shape[1] * lax.axis_size("tp")
    square_sum = of_everyone(jnp.sum(floats * floats, axis=1), "tp")
    inv_rms = lax.rsqrt(square_sum / full_width + EPSILON)
    return (floats * inv_rms[:, None] * finishing_rms_gains[None, :]).astype(jnp.bfloat16)


def solution(mesh):
    return jax.shard_map(
        on_device,
        mesh=mesh,
        in_specs=(
            P(("grp", "sp"), "tp"),
            P(None, "sp", "tp"),
            P(None, "sp", "tp"),
            P(None, None, "tp"),
            P(None, "tp", None, None),
            P(None, "tp", None, None),
            P(None, "tp"),
            P(("grp", "sp")),
            P(("grp", "sp"), "tp"),
            P(None, "tp", "sp"),
            P(),
            P("tp"),
        ),
        out_specs=P(("grp", "sp"), "tp"),
        check_vma=False,
    )
```

profile of v0, /device:TPU:33, one launch (start us, length us, event | category | flops | bytes accessed | tf_op | source)
XLA Modules:
  0.0 602.2 jit_solution(12787368369105031495)
XLA Ops:
  6.6 0.8 slice_bitcast_fusion
  7.4 0.6 pad_maximum_fusion.10
  8.1 1.4 fusion.135
  9.6 1.1 copy.23
  10.7 1.3 broadcast_in_dim.6
  12.0 45.1 %all-to-all-start = ((bf16[8,384,256]{1,2,0:T(8,128)(2,1)}), bf16[8,384,256]{1,2,0:T(8,128)(2,1)S(1)}, u32[]{:S(2)}, u32[]{:S(2)}) async-start(bf16[8,384,256]{1,2,0:T(8,128)(2,1)} %broadcast_in_dim.6), calls=%async_computation | async-start | bytes 3145728 | tf_op jit(solution)/shard_map/all_to_all | solution.py:13
  57.1 0.6 pad_maximum_fusion.11
  59.1 18.7 %all-to-all-done = bf16[8,384,256]{1,2,0:T(8,128)(2,1)S(1)} async-done(((bf16[8,384,256]{1,2,0:T(8,128)(2,1)}), bf16[8,384,256]{1,2,0:T(8,128)(2,1)S(1)}, u32[]{:S(2)}, u32[]{:S(2)}) %all-to-all-start) | async-done | bytes 1572896 | tf_op jit(solution)/shard_map/all_to_all | solution.py:13
  78.6 72.2 %all-gather.11.cloned.1.call-done = bf16[2048,512]{1,0:T(8,128)(2,1)} async-done(((bf16[64,512]{1,0:T(8,128)(2,1)}), bf16[2048,512]{1,0:T(8,128)(2,1)}) %all-gather.11.cloned.1.call-update) | async-done | bytes 2097168 | tf_op jit(solution)/shard_map/all_gather | solution.py:30
  150.8 1.8 convolution_convert_fusion.4
  152.7 1.7 collective-permute-start
  154.4 0.7 collective-permute-done
  167.4 0.7 fusion.115
  168.1 0.7 pad_maximum_fusion.29
  168.8 0.6 pad_maximum_fusion.28
  169.5 0.7 fusion.112
  170.2 0.7 pad_maximum_fusion.25
  170.9 0.7 pad_maximum_fusion.24
  171.6 0.6 pad_maximum_fusion.21
  172.6 0.7 pad_maximum_fusion.13
  174.2 1.5 pad.227
  176.5 0.7 slice_add_fusion.5
  177.4 40.9 %all-gather.4 = f32[32,2,256]{2,1,0:T(2,128)S(1)} all-gather(f32[1,2,256]{2,1,0:T(2,128)S(1)} %maximum_bitcast_fusion), channel_id=2, replica_groups=mesh['grp'=2,'sp'=32,'tp'=8] {'sp'}, dimensions={0}, use_global_device_ids=true | all-gather | bytes 67584 | tf_op jit(solution)/shard_map/all_gather | solution.py:48
  218.4 59.8 %all-gather.15.cloned.1.call-done = bf16[1,256,2048]{1,2,0:T(8,128)(2,1)} async-done(((bf16[1,256,64]{1,2,0:T(8,128)(2,1)}), bf16[1,256,2048]{1,2,0:T(8,128)(2,1)}) %all-gather.15.cloned.1.call-update) | async-done | bytes 1048592 | tf_op jit(solution)/shard_map/all_gather | solution.py:98
  278.2 3.8 convolution_convert_fusion.1
  282.1 46.2 %all_to_all.26 = bf16[8,384,256]{2,1,0:T(8,128)(2,1)S(1)} all-to-all(bf16[8,384,256]{2,1,0:T(8,128)(2,1)S(1)} %bitcast.108), channel_id=1, replica_groups=mesh['grp'=2,'sp'=32,'tp'=8] {'tp'}, dimensions={0} | all-to-all | bytes 3145728 | tf_op jit(solution)/shard_map/all_to_all | solution.py:77
  328.6 0.7 copy-done.2
  329.5 1.3 broadcast_in_dim.7
  330.8 4.5 all-to-all-start.2
  335.9 20.1 %all-to-all-done.2 = bf16[8,384,256]{1,2,0:T(8,128)(2,1)S(1)} async-done(((bf16[8,384,256]{1,2,0:T(8,128)(2,1)}), bf16[8,384,256]{1,2,0:T(8,128)(2,1)S(1)}, u32[]{:S(2)}, u32[]{:S(2)}) %all-to-all-start.2) | async-done | bytes 1572896 | tf_op jit(solution)/shard_map/all_to_all | solution.py:13
  356.9 52.8 %all-gather.13.cloned.1.call-done = bf16[2048,512]{1,0:T(8,128)(2,1)} async-done(((bf16[64,512]{1,0:T(8,128)(2,1)}), bf16[2048,512]{1,0:T(8,128)(2,1)}) %all-gather.13.cloned.1.call-update) | async-done | bytes 2097168 | tf_op jit(solution)/shard_map/all_gather | solution.py:30
  409.7 1.8 convolution_convert_fusion.2
  411.6 1.5 collective-permute-start.1
  414.2 1.3 fusion.22
  415.9 0.8 slice.719
  416.7 1.0 multiply_add_fusion.2
  423.5 0.6 slice.763
  425.3 0.6 slice.765
  427.0 0.6 slice.732
  427.7 0.6 slice.767
  429.4 0.6 slice.726
  430.1 0.6 slice.769
  434.2 0.7 multiply_add_fusion.14
  435.0 0.7 fusion.120
  435.7 0.6 pad_maximum_fusion.31
  436.4 0.6 pad_maximum_fusion.30
  437.0 0.7 fusion.111
  437.8 0.6 pad_maximum_fusion.27
  438.4 0.7 pad_maximum_fusion.26
  439.1 0.7 fusion.109
  439.9 0.7 pad_maximum_fusion.23
  440.9 0.8 fusion.105
  441.7 0.6 pad_maximum_fusion.15
  442.4 0.6 pad_maximum_fusion.14
  443.3 1.6 pad.259
  445.6 0.7 slice_add_fusion.1
  446.4 1.7 pad.242
  448.1 0.7 slice_add_fusion
  448.8 41.6 %all-gather.5 = f32[32,2,256]{2,1,0:T(2,128)S(1)} all-gather(f32[1,2,256]{2,1,0:T(2,128)S(1)} %maximum_bitcast_fusion.1), channel_id=4, replica_groups=mesh['grp'=2,'sp'=32,'tp'=8] {'sp'}, dimensions={0}, use_global_device_ids=true | all-gather | bytes 67584 | tf_op jit(solution)/shard_map/all_gather | solution.py:48
  490.5 45.1 %all-gather.17.cloned.1.call-done = bf16[1,256,2048]{1,2,0:T(8,128)(2,1)} async-done(((bf16[1,256,64]{1,2,0:T(8,128)(2,1)}), bf16[1,256,2048]{1,2,0:T(8,128)(2,1)}) %all-gather.17.cloned.1.call-update) | async-done | bytes 1048592 | tf_op jit(solution)/shard_map/all_gather | solution.py:98
  535.7 3.9 convolution_convert_fusion
  539.7 46.7 %all_to_all.27 = bf16[8,384,256]{2,1,0:T(8,128)(2,1)S(1)} all-to-all(bf16[8,384,256]{2,1,0:T(8,128)(2,1)S(1)} %bitcast.109), channel_id=1, replica_groups=mesh['grp'=2,'sp'=32,'tp'=8] {'tp'}, dimensions={0} | all-to-all | bytes 3145728 | tf_op jit(solution)/shard_map/all_to_all | solution.py:77
  586.7 8.1 %all_to_all.28 = f32[8,1,384]{2,1,0:T(1,128)S(1)} all-to-all(f32[8,1,384]{2,1,0:T(1,128)S(1)} %broadcast_in_dim.8), channel_id=1, replica_groups=mesh['grp'=2,'sp'=32,'tp'=8] {'tp'}, dimensions={0} | all-to-all | bytes 24576 | tf_op jit(solution)/shard_map/all_to_all | solution.py:13
  594.9 0.8 fusion.36
  (356 shorter events, 34.4 us)
Async XLA Ops:
  6.5 144.2 %all-gather.11.cloned.1.call-start = ((), (), s32[]{:S(2)}) async-start(), calls=%async_computation.5 | async-start | bytes 2162688 | tf_op jit(solution)/shard_map/all_gather | solution.py:30
  8.1 270.1 %all-gather.15.cloned.1.call-start = ((), (), s32[]{:S(2)}) async-start(), calls=%async_computation.7 | async-start | bytes 1081344 | tf_op jit(solution)/shard_map/all_gather | solution.py:98
  12.0 45.8 %copy-start.28 = (f32[2,256]{1,0:T(2,128)S(1)}, f32[2,256]{1,0:T(2,128)}, u32[]{:S(2)}) copy-start(f32[2,256]{1,0:T(2,128)} %param.22) | copy-start | bytes 6148
  12.0 46.4 %copy-start.11 = (bf16[2,4,256]{2,1,0:T(4,128)(2,1)S(1)}, bf16[2,4,256]{2,1,0:T(4,128)(2,1)}, u32[]{:S(2)}) copy-start(bf16[2,4,256]{2,1,0:T(4,128)(2,1)} %param.19) | copy-start | bytes 12292
  12.0 47.0 %copy-start.10 = (f32[2,2048]{1,0:T(2,128)S(1)}, f32[2,2048]{1,0:T(2,128)}, u32[]{:S(2)}) copy-start(f32[2,2048]{1,0:T(2,128)} %param.26) | copy-start | bytes 49156
  12.0 65.7 %all-to-all-start = ((bf16[8,384,256]{1,2,0:T(8,128)(2,1)}), bf16[8,384,256]{1,2,0:T(8,128)(2,1)S(1)}, u32[]{:S(2)}, u32[]{:S(2)}) async-start(bf16[8,384,256]{1,2,0:T(8,128)(2,1)} %broadcast_in_dim.6), calls=%async_computation | async-start | bytes 3145728 | tf_op jit(solution)/shard_map/all_to_all | solution.py:13
  57.1 352.6 %all-gather.13.cloned.1.call-start = ((), (), s32[]{:S(2)}) async-start(), calls=%async_computation.6 | async-start | bytes 2162688 | tf_op jit(solution)/shard_map/all_gather | solution.py:30
  78.6 76.7 %copy-start.31 = (f32[384,256]{1,0:T(8,128)S(1)}, f32[384,256]{1,0:T(8,128)}, u32[]{:S(2)}) copy-start(f32[384,256]{1,0:T(8,128)} %param.24) | copy-start | bytes 1179652
  78.6 76.7 %copy-start.33 = (bf16[2,1,256,256]{3,2,1,0:T(8,128)(2,1)S(1)}, bf16[2,1,256,256]{3,2,1,0:T(8,128)(2,1)}, u32[]{:S(2)}) copy-start(bf16[2,1,256,256]{3,2,1,0:T(8,128)(2,1)} %param.20) | copy-start | bytes 786436
  78.6 76.7 %copy-start.36 = (f32[384]{0:T(512)S(1)}, f32[384]{0:T(512)}, u32[]{:S(2)}) copy-start(f32[384]{0:T(512)} %param.23) | copy-start | bytes 4612
  152.6 3.0 copy-start.35
  152.7 2.5 collective-permute-start
  156.1 11.2 %copy-start = (f32[384,256]{1,0:T(8,128)}, f32[384,256]{1,0:T(8,128)S(1)}, u32[]{:S(2)}) copy-start(f32[384,256]{1,0:T(8,128)S(1)} %fusion.25) | copy-start | bytes 1179652
  165.6 6.7 %copy-start.26 = (f32[1,256]{1,0:T(1,128)S(1)}, f32[1,256]{1,0:T(1,128)}, u32[]{:S(2)}) copy-start(f32[1,256]{1,0:T(1,128)} %slice.803) | copy-start | bytes 3076
  165.6 6.8 %copy-start.24 = (f32[1,256]{1,0:T(1,128)S(1)}, f32[1,256]{1,0:T(1,128)}, u32[]{:S(2)}) copy-start(f32[1,256]{1,0:T(1,128)} %slice.828) | copy-start | bytes 3076
  165.6 6.9 %copy-start.22 = (f32[1,256]{1,0:T(1,128)S(1)}, f32[1,256]{1,0:T(1,128)}, u32[]{:S(2)}) copy-start(f32[1,256]{1,0:T(1,128)} %slice.802) | copy-start | bytes 3076
  172.4 1.6 copy-start.20
  174.0 1.8 copy-start.18
  175.7 0.6 copy-start.16
  175.9 1.4 slice-start
  176.5 101.7 %copy-start.5 = (f32[384,256]{1,0:T(8,128)}, f32[384,256]{1,0:T(8,128)S(1)}, u32[]{:S(2)}) copy-start(f32[384,256]{1,0:T(8,128)S(1)} %pad.226) | copy-start | bytes 1179652
  177.2 101.0 %copy-start.6 = (f32[384,256]{1,0:T(8,128)}, f32[384,256]{1,0:T(8,128)S(1)}, u32[]{:S(2)}) copy-start(f32[384,256]{1,0:T(8,128)S(1)} %pad.211) | copy-start | bytes 1179652
  328.3 0.9 copy-start.2
  330.8 25.2 %all-to-all-start.2 = ((bf16[8,384,256]{1,2,0:T(8,128)(2,1)}), bf16[8,384,256]{1,2,0:T(8,128)(2,1)S(1)}, u32[]{:S(2)}, u32[]{:S(2)}) async-start(bf16[8,384,256]{1,2,0:T(8,128)(2,1)} %broadcast_in_dim.7), calls=%async_computation.2 | async-start | bytes 3145728 | tf_op jit(solution)/shard_map/all_to_all | solution.py:13
  335.3 200.3 %all-gather.17.cloned.1.call-start = ((), (), s32[]{:S(2)}) async-start(), calls=%async_computation.8 | async-start | bytes 1081344 | tf_op jit(solution)/shard_map/all_gather | solution.py:98
  356.8 56.7 %copy-start.12 = (f32[1,1,256]{2,1,0:T(1,128)S(1)}, f32[1,1,256]{2,1,0:T(1,128)}, u32[]{:S(2)}) copy-start(f32[1,1,256]{2,1,0:T(1,128)} %get-tuple-element.193) | copy-start | bytes 3076
  356.9 56.7 %copy-start.13 = (f32[1,1,256]{2,1,0:T(1,128)S(1)}, f32[1,1,256]{2,1,0:T(1,128)}, u32[]{:S(2)}) copy-start(f32[1,1,256]{2,1,0:T(1,128)} %get-tuple-element.194) | copy-start | bytes 3076
  356.9 56.7 %copy-start.14 = (f32[1,1,256]{2,1,0:T(1,128)S(1)}, f32[1,1,256]{2,1,0:T(1,128)}, u32[]{:S(2)}) copy-start(f32[1,1,256]{2,1,0:T(1,128)} %get-tuple-element.199) | copy-start | bytes 3076
  356.9 56.7 %copy-start.15 = (f32[1,1,256]{2,1,0:T(1,128)S(1)}, f32[1,1,256]{2,1,0:T(1,128)}, u32[]{:S(2)}) copy-start(f32[1,1,256]{2,1,0:T(1,128)} %get-tuple-element.200) | copy-start | bytes 3076
  356.9 56.9 %copy-start.30 = (f32[1,256]{1,0:T(1,128)S(1)}, f32[1,256]{1,0:T(1,128)}, u32[]{:S(2)}) copy-start(f32[1,256]{1,0:T(1,128)} %get-tuple-element.209) | copy-start | bytes 3076
  356.9 56.9 %copy-start.32 = (f32[384,256]{1,0:T(8,128)S(1)}, f32[384,256]{1,0:T(8,128)}, u32[]{:S(2)}) copy-start(f32[384,256]{1,0:T(8,128)} %param.24) | copy-start | bytes 1179652
  356.9 56.9 %copy-start.34 = (bf16[2,1,256,256]{3,2,1,0:T(8,128)(2,1)S(1)}, bf16[2,1,256,256]{3,2,1,0:T(8,128)(2,1)}, u32[]{:S(2)}) copy-start(bf16[2,1,256,256]{3,2,1,0:T(8,128)(2,1)} %param.20) | copy-start | bytes 786436
  356.9 56.9 %copy-start.37 = (f32[384]{0:T(512)S(1)}, f32[384]{0:T(512)}, u32[]{:S(2)}) copy-start(f32[384]{0:T(512)} %param.23) | copy-start | bytes 4612
  411.6 2.0 collective-permute-start.1
  415.5 18.7 %copy-start.1 = (f32[384,256]{1,0:T(8,128)}, f32[384,256]{1,0:T(8,128)S(1)}, u32[]{:S(2)}) copy-start(f32[384,256]{1,0:T(8,128)S(1)} %fusion.22) | copy-start | bytes 1179652
  432.5 8.1 %copy-start.27 = (f32[1,256]{1,0:T(1,128)S(1)}, f32[1,256]{1,0:T(1,128)}, u32[]{:S(2)}) copy-start(f32[1,256]{1,0:T(1,128)} %slice.862) | copy-start | bytes 3076
  432.5 8.2 %copy-start.8 = (f32[23,256]{1,0:T(8,128)S(1)}, f32[23,256]{1,0:T(8,128)}, u32[]{:S(2)}) copy-start(f32[23,256]{1,0:T(8,128)} %slice.732) | copy-start | bytes 70660
  432.5 8.2 %copy-start.9 = (f32[23,256]{1,0:T(8,128)S(1)}, f32[23,256]{1,0:T(8,128)}, u32[]{:S(2)}) copy-start(f32[23,256]{1,0:T(8,128)} %slice.767) | copy-start | bytes 70660
  432.5 8.2 %copy-start.25 = (f32[1,256]{1,0:T(1,128)S(1)}, f32[1,256]{1,0:T(1,128)}, u32[]{:S(2)}) copy-start(f32[1,256]{1,0:T(1,128)} %slice.887) | copy-start | bytes 3076
  432.5 8.3 %copy-start.23 = (f32[1,256]{1,0:T(1,128)S(1)}, f32[1,256]{1,0:T(1,128)}, u32[]{:S(2)}) copy-start(f32[1,256]{1,0:T(1,128)} %slice.861) | copy-start | bytes 3076
  432.5 8.4 %copy-start.7 = (f32[47,256]{1,0:T(8,128)S(1)}, f32[47,256]{1,0:T(8,128)}, u32[]{:S(2)}) copy-start(f32[47,256]{1,0:T(8,128)} %slice.769) | copy-start | bytes 144388
  440.7 2.4 copy-start.21
  443.1 1.8 copy-start.19
  444.9 0.7 copy-start.17
  445.0 1.4 slice-start.1
  445.6 90.0 %copy-start.3 = (f32[384,256]{1,0:T(8,128)}, f32[384,256]{1,0:T(8,128)S(1)}, u32[]{:S(2)}) copy-start(f32[384,256]{1,0:T(8,128)S(1)} %pad.258) | copy-start | bytes 1179652
  446.4 89.3 %copy-start.4 = (f32[384,256]{1,0:T(8,128)}, f32[384,256]{1,0:T(8,128)S(1)}, u32[]{:S(2)}) copy-start(f32[384,256]{1,0:T(8,128)S(1)} %pad.243) | copy-start | bytes 1179652
  586.3 8.5 %copy-start.29 = (f32[256]{0:T(256)S(1)}, f32[256]{0:T(256)}, u32[]{:S(2)}) copy-start(f32[256]{0:T(256)} %param.27) | copy-start | bytes 3076
Sparse Core Ops, SparseCore 0:
  9.4 141.3 all-gather.10
  152.9 125.2 all-gather.14
  280.3 129.3 all-gather.12
  411.6 123.9 all-gather.16
where the time goes:
time: 604 us; the launch traced here: 602 us
  waiting for transfers between devices  271 us (45%)
  blocking collectives  183 us (30%)
  starting transfers between devices  52.9 us (9%)
  local copies, waits for them, and re-layouts  42.2 us (7%)
  other arithmetic  24.4 us (4%)
  between operations  14.8 us (2%)
  matrix products  13.7 us (2%)
    all_gather x2, waiting for transfers between devices, in_one_piece(): whole = lax.all_gather(both, axis, axis=dim, tiled=True)  125 us
    all_gather x2, waiting for transfers between devices, fetch_layer(): lax.all_gather(exit_projector_matrix[tier_number], 'sp', axis=1, tiled=True)  105 us
    all_to_all x2, blocking collectives, summed_on_arrival(): lax.all_to_all(tiles, axis, split_axis=0, concat_axis=0, tiled=True)  92.9 us
    all_gather x2, blocking collectives, gathered_once(): both, at, found = (lax.all_gather(jnp.concatenate(lines), axis), 0, {})  82.5 us
    all_to_all x2, starting transfers between devices, sent_to_all(): return lax.all_to_all(copies, axis, split_axis=0, concat_axis=0, tiled=True)  49.6 us
    all_to_all x2, waiting for transfers between devices, sent_to_all(): return lax.all_to_all(copies, axis, split_axis=0, concat_axis=0, tiled=True)  38.8 us
    slice x114, local copies, waits for them, and re-layouts, on_device(): lax.associative_scan(combine_pairs, (keep_rate, driven), axis=0)  28.4 us
  transfers between devices with their start and end apart: 8, of which 8 were waited for; matrix products, arithmetic and copies ran while one was open for 12% of the time, Pallas kernels for 0%

commit v1 on v0

--- a/solution.py
+++ b/solution.py
@@ -95,7 +95,12 @@
     in_pair = in_one_piece(
         (multiplier_matrix[tier_number], memory_path_matrix[tier_number]), "sp", 0, 1
     )
-    out_full = lax.all_gather(exit_projector_matrix[tier_number], "sp", axis=1, tiled=True)
+    out_full = jnp.concatenate(
+        lax.all_to_all(
+            jnp.stack([exit_projector_matrix[tier_number]] * lax.axis_size("sp")), "sp", 0, 0
+        ),
+        axis=1,
+    )
     return (in_pair[0], in_pair[1], out_full)
 
 

time: 604 us -> 647 us (1.071)
  starting transfers between devices: 52.9 us -> 108 us
  blocking collectives: 183 us -> 167 us
    all_gather x2, waiting for transfers between devices: 125 us -> 233 us  [in_one_piece(): whole = lax.all_gather(both, axis, axis=dim, tiled=True)]
    all_gather x2 -> x0, waiting for transfers between devices: 105 us -> none  [fetch_layer(): lax.all_gather(exit_projector_matrix[tier_number], 'sp', axis=1, tiled=True)]
    all_to_all x0 -> x3, starting transfers between devices: none -> 56.2 us  [the longest x1 33.9 us: summed_on_arrival(): lax.all_to_all(tiles, axis, split_axis=0, concat_axis=0, tiled=True)]
    all_to_all x2 -> x1, blocking collectives: 92.9 us -> 53.9 us  [summed_on_arrival(): lax.all_to_all(tiles, axis, split_axis=0, concat_axis=0, tiled=True)]
    all_to_all x1 -> x2, blocking collectives: 8.1 us -> 32.1 us  [sent_to_all(): return lax.all_to_all(copies, axis, split_axis=0, concat_axis=0, tiled=True)]
    all_to_all x2 -> x1, waiting for transfers between devices: 38.8 us -> 18.9 us  [sent_to_all(): return lax.all_to_all(copies, axis, split_axis=0, concat_axis=0, tiled=True)]
    all_to_all x0 -> x3, waiting for transfers between devices: none -> 19.8 us  [the longest x1 19.8 us: summed_on_arrival(): lax.all_to_all(tiles, axis, split_axis=0, concat_axis=0, tiled=True)]
    all_to_all x2 -> x1, starting transfers between devices: 49.6 us -> 45.1 us  [sent_to_all(): return lax.all_to_all(copies, axis, split_axis=0, concat_axis=0, tiled=True)]
  transfers between devices with their start and end apart: 8 -> 8, of which waited for: 8 -> 6; matrix products, arithmetic and copies ran while one was open for 12% -> 11% of each run, Pallas kernels for 0% -> 0%
where the time goes in v1:
time: 647 us; the launch traced here: 645 us
  waiting for transfers between devices  273 us (42%)
  blocking collectives  167 us (26%)
  starting transfers between devices  108 us (17%)
  local copies, waits for them, and re-layouts  43.6 us (7%)
  other arithmetic  24.3 us (4%)
  between operations  15.2 us (2%)
  matrix products  13.8 us (2%)
    all_gather x2, waiting for transfers between devices, in_one_piece(): whole = lax.all_gather(both, axis, axis=dim, tiled=True)  233 us
    all_gather x2, blocking collectives, gathered_once(): both, at, found = (lax.all_gather(jnp.concatenate(lines), axis), 0, {})  80.6 us
    all_to_all x1, blocking collectives, summed_on_arrival(): lax.all_to_all(tiles, axis, split_axis=0, concat_axis=0, tiled=True)  53.9 us
    all_to_all x1, starting transfers between devices, sent_to_all(): return lax.all_to_all(copies, axis, split_axis=0, concat_axis=0, tiled=True)  45.1 us
    all_to_all x1, starting transfers between devices, summed_on_arrival(): lax.all_to_all(tiles, axis, split_axis=0, concat_axis=0, tiled=True)  33.9 us
    all_to_all x2, blocking collectives, sent_to_all(): return lax.all_to_all(copies, axis, split_axis=0, concat_axis=0, tiled=True)  32.1 us
    slice x114, local copies, waits for them, and re-layouts, on_device(): lax.associative_scan(combine_pairs, (keep_rate, driven), axis=0)  28.3 us
    all_to_all x2, starting transfers between devices, fetch_layer(): lax.all_to_all(jnp.stack([exit_projector_matrix[tier_number]] * lax.axis_...  22.3 us
  transfers between devices with their start and end apart: 8, of which 6 were waited for; matrix products, arithmetic and copies ran while one was open for 11% of the time, Pallas kernels for 0%

profile of v1, /device:TPU:33, one launch (start us, length us, event | category | flops | bytes accessed | tf_op | source)
XLA Modules:
  0.0 644.9 jit_solution(461318313953870708)
XLA Ops:
  6.6 1.4 slice_bitcast_fusion.1
  8.0 0.6 pad_maximum_fusion.10
  8.7 1.1 copy.25
  9.8 1.3 broadcast_in_dim.6
  11.1 45.1 %all-to-all-start = ((bf16[8,384,256]{1,2,0:T(8,128)(2,1)}), bf16[8,384,256]{1,2,0:T(8,128)(2,1)S(1)}, u32[]{:S(2)}, u32[]{:S(2)}) async-start(bf16[8,384,256]{1,2,0:T(8,128)(2,1)} %broadcast_in_dim.6), calls=%async_computation | async-start | bytes 3145728 | tf_op jit(solution)/shard_map/all_to_all | solution.py:13
  57.9 18.9 %all-to-all-done = bf16[8,384,256]{1,2,0:T(8,128)(2,1)S(1)} async-done(((bf16[8,384,256]{1,2,0:T(8,128)(2,1)}), bf16[8,384,256]{1,2,0:T(8,128)(2,1)S(1)}, u32[]{:S(2)}, u32[]{:S(2)}) %all-to-all-start) | async-done | bytes 1572896 | tf_op jit(solution)/shard_map/all_to_all | solution.py:13
  76.8 1.1 stack.6
  77.9 6.5 %all-to-all-start.1 = ((bf16[32,256,64]{1,2,0:T(8,128)(2,1)}), bf16[32,256,64]{1,2,0:T(8,128)(2,1)}, u32[]{:S(2)}, u32[]{:S(2)}) async-start(bf16[32,256,64]{1,2,0:T(8,128)(2,1)} %stack.6), calls=%async_computation.1 | async-start | bytes 2097152 | tf_op jit(solution)/shard_map/all_to_all | solution.py:99
  85.3 124.7 %all-gather.7.cloned.1.call-done = bf16[2048,512]{1,0:T(8,128)(2,1)} async-done(((bf16[64,512]{1,0:T(8,128)(2,1)}), bf16[2048,512]{1,0:T(8,128)(2,1)}) %all-gather.7.cloned.1.call-update) | async-done | bytes 2097168 | tf_op jit(solution)/shard_map/all_gather | solution.py:30
  210.0 1.8 convolution_convert_fusion.4
  211.9 2.6 collective-permute-start
  214.5 0.7 collective-permute-done
  227.5 0.7 fusion.113
  228.2 0.7 pad_maximum_fusion.29
  229.0 0.7 pad_maximum_fusion.28
  229.7 0.7 fusion.110
  230.4 0.6 pad_maximum_fusion.25
  231.0 0.6 pad_maximum_fusion.24
  231.8 0.7 pad_maximum_fusion.21
  232.7 0.7 pad_maximum_fusion.13
  233.5 0.6 pad_maximum_fusion.12
  234.4 1.6 pad.227
  236.8 0.7 slice_add_fusion.5
  237.6 40.9 %all-gather.2 = f32[32,2,256]{2,1,0:T(2,128)S(1)} all-gather(f32[1,2,256]{2,1,0:T(2,128)S(1)} %maximum_bitcast_fusion), channel_id=2, replica_groups=mesh['grp'=2,'sp'=32,'tp'=8] {'sp'}, dimensions={0}, use_global_device_ids=true | all-gather | bytes 67584 | tf_op jit(solution)/shard_map/all_gather | solution.py:48
  278.6 3.8 convolution_convert_fusion.1
  282.4 1.3 copy.44
  283.7 33.9 %all-to-all-start.2 = ((bf16[8,384,256]{2,1,0:T(8,128)(2,1)}), bf16[8,384,256]{2,1,0:T(8,128)(2,1)S(1)}, u32[]{:S(2)}, u32[]{:S(2)}) async-start(bf16[8,384,256]{2,1,0:T(8,128)(2,1)} %bitcast.101), calls=%async_computation.2 | async-start | bytes 3145728 | tf_op jit(solution)/shard_map/all_to_all | solution.py:77
  317.6 0.6 pad_maximum_fusion.11
  318.3 19.8 %all-to-all-done.2 = bf16[8,384,256]{2,1,0:T(8,128)(2,1)S(1)} async-done(((bf16[8,384,256]{2,1,0:T(8,128)(2,1)}), bf16[8,384,256]{2,1,0:T(8,128)(2,1)S(1)}, u32[]{:S(2)}, u32[]{:S(2)}) %all-to-all-start.2) | async-done | bytes 1572896 | tf_op jit(solution)/shard_map/all_to_all | solution.py:77
  338.7 24.0 %all_to_all.36 = bf16[8,384,256]{1,2,0:T(8,128)(2,1)S(1)} all-to-all(bf16[8,384,256]{1,2,0:T(8,128)(2,1)S(1)} %broadcast_in_dim.7), channel_id=1, replica_groups=mesh['grp'=2,'sp'=32,'tp'=8] {'tp'}, dimensions={0} | all-to-all | bytes 3145728 | tf_op jit(solution)/shard_map/all_to_all | solution.py:13
  362.8 1.1 stack.7
  363.9 15.8 %all-to-all-start.4 = ((bf16[32,256,64]{1,2,0:T(8,128)(2,1)}), bf16[32,256,64]{1,2,0:T(8,128)(2,1)}, u32[]{:S(2)}, u32[]{:S(2)}) async-start(bf16[32,256,64]{1,2,0:T(8,128)(2,1)} %stack.7), calls=%async_computation.4 | async-start | bytes 2097152 | tf_op jit(solution)/shard_map/all_to_all | solution.py:99
  380.6 108.4 %all-gather.9.cloned.1.call-done = bf16[2048,512]{1,0:T(8,128)(2,1)} async-done(((bf16[64,512]{1,0:T(8,128)(2,1)}), bf16[2048,512]{1,0:T(8,128)(2,1)}) %all-gather.9.cloned.1.call-update) | async-done | bytes 2097168 | tf_op jit(solution)/shard_map/all_gather | solution.py:30
  489.1 1.8 convolution_convert_fusion.2
  490.9 4.0 collective-permute-start.1
  494.9 0.7 collective-permute-done.1
  496.2 1.3 fusion.22
  498.0 0.8 slice.724
  498.7 1.0 multiply_add_fusion.2
  509.1 0.6 slice.737
  509.7 0.6 slice.772
  511.5 0.6 slice.731
  512.1 0.6 slice.774
  516.2 0.7 multiply_add_fusion.14
  517.0 0.7 fusion.118
  517.7 0.7 pad_maximum_fusion.31
  518.5 0.6 pad_maximum_fusion.30
  519.1 0.7 fusion.109
  519.8 0.7 pad_maximum_fusion.27
  520.5 0.7 pad_maximum_fusion.26
  521.2 0.7 fusion.107
  522.0 0.7 pad_maximum_fusion.23
  523.0 0.8 fusion.103
  523.8 0.6 pad_maximum_fusion.15
  524.5 0.6 pad_maximum_fusion.14
  525.3 1.6 pad.259
  527.8 1.7 pad.242
  529.5 0.7 slice_add_fusion.1
  530.2 0.7 slice_add_fusion
  530.9 39.7 %all-gather.3 = f32[32,2,256]{2,1,0:T(2,128)S(1)} all-gather(f32[1,2,256]{2,1,0:T(2,128)S(1)} %maximum_bitcast_fusion.1), channel_id=3, replica_groups=mesh['grp'=2,'sp'=32,'tp'=8] {'sp'}, dimensions={0}, use_global_device_ids=true | all-gather | bytes 67584 | tf_op jit(solution)/shard_map/all_gather | solution.py:48
  570.8 3.9 convolution_convert_fusion
  574.8 53.9 %all_to_all.37 = bf16[8,384,256]{2,1,0:T(8,128)(2,1)S(1)} all-to-all(bf16[8,384,256]{2,1,0:T(8,128)(2,1)S(1)} %bitcast.114), channel_id=1, replica_groups=mesh['grp'=2,'sp'=32,'tp'=8] {'tp'}, dimensions={0} | all-to-all | bytes 3145728 | tf_op jit(solution)/shard_map/all_to_all | solution.py:77
  629.1 8.1 %all_to_all.38 = f32[8,1,384]{2,1,0:T(1,128)S(1)} all-to-all(f32[8,1,384]{2,1,0:T(1,128)S(1)} %broadcast_in_dim.8), channel_id=1, replica_groups=mesh['grp'=2,'sp'=32,'tp'=8] {'tp'}, dimensions={0} | all-to-all | bytes 24576 | tf_op jit(solution)/shard_map/all_to_all | solution.py:13
  637.2 0.8 fusion.34
  (364 shorter events, 34.4 us)
Async XLA Ops:
  6.5 203.5 %all-gather.7.cloned.1.call-start = ((), (), s32[]{:S(2)}) async-start(), calls=%async_computation.7 | async-start | bytes 2162688 | tf_op jit(solution)/shard_map/all_gather | solution.py:30
  11.1 45.1 %copy-start.32 = (f32[2,256]{1,0:T(2,128)S(1)}, f32[2,256]{1,0:T(2,128)}, u32[]{:S(2)}) copy-start(f32[2,256]{1,0:T(2,128)} %param.22) | copy-start | bytes 6148
  11.1 45.6 %copy-start.15 = (bf16[2,4,256]{2,1,0:T(4,128)(2,1)S(1)}, bf16[2,4,256]{2,1,0:T(4,128)(2,1)}, u32[]{:S(2)}) copy-start(bf16[2,4,256]{2,1,0:T(4,128)(2,1)} %param.19) | copy-start | bytes 12292
  11.1 46.2 %copy-start.13 = (bf16[2,256,64]{1,2,0:T(8,128)(2,1)S(1)}, bf16[2,256,64]{1,2,0:T(8,128)(2,1)}, u32[]{:S(2)}) copy-start(bf16[2,256,64]{1,2,0:T(8,128)(2,1)} %param.25) | copy-start | bytes 196612
  11.1 46.8 %copy-start.14 = (f32[2,2048]{1,0:T(2,128)S(1)}, f32[2,2048]{1,0:T(2,128)}, u32[]{:S(2)}) copy-start(f32[2,2048]{1,0:T(2,128)} %param.26) | copy-start | bytes 49156
  11.1 65.7 %all-to-all-start = ((bf16[8,384,256]{1,2,0:T(8,128)(2,1)}), bf16[8,384,256]{1,2,0:T(8,128)(2,1)S(1)}, u32[]{:S(2)}, u32[]{:S(2)}) async-start(bf16[8,384,256]{1,2,0:T(8,128)(2,1)} %broadcast_in_dim.6), calls=%async_computation | async-start | bytes 3145728 | tf_op jit(solution)/shard_map/all_to_all | solution.py:13
  77.9 200.6 %all-to-all-start.1 = ((bf16[32,256,64]{1,2,0:T(8,128)(2,1)}), bf16[32,256,64]{1,2,0:T(8,128)(2,1)}, u32[]{:S(2)}, u32[]{:S(2)}) async-start(bf16[32,256,64]{1,2,0:T(8,128)(2,1)} %stack.6), calls=%async_computation.1 | async-start | bytes 2097152 | tf_op jit(solution)/shard_map/all_to_all | solution.py:99
  85.3 130.2 %copy-start.35 = (f32[384,256]{1,0:T(8,128)S(1)}, f32[384,256]{1,0:T(8,128)}, u32[]{:S(2)}) copy-start(f32[384,256]{1,0:T(8,128)} %param.24) | copy-start | bytes 1179652
  85.3 130.2 %copy-start.37 = (bf16[2,1,256,256]{3,2,1,0:T(8,128)(2,1)S(1)}, bf16[2,1,256,256]{3,2,1,0:T(8,128)(2,1)}, u32[]{:S(2)}) copy-start(bf16[2,1,256,256]{3,2,1,0:T(8,128)(2,1)} %param.20) | copy-start | bytes 786436
  85.3 130.2 %copy-start.40 = (f32[384]{0:T(512)S(1)}, f32[384]{0:T(512)}, u32[]{:S(2)}) copy-start(f32[384]{0:T(512)} %param.23) | copy-start | bytes 4612
  211.9 3.9 copy-start.39
  211.9 3.3 collective-permute-start
  216.3 11.2 %copy-start = (f32[384,256]{1,0:T(8,128)}, f32[384,256]{1,0:T(8,128)S(1)}, u32[]{:S(2)}) copy-start(f32[384,256]{1,0:T(8,128)S(1)} %fusion.25) | copy-start | bytes 1179652
  225.7 6.7 %copy-start.30 = (f32[1,256]{1,0:T(1,128)S(1)}, f32[1,256]{1,0:T(1,128)}, u32[]{:S(2)}) copy-start(f32[1,256]{1,0:T(1,128)} %slice.809) | copy-start | bytes 3076
  225.7 6.8 %copy-start.28 = (f32[1,256]{1,0:T(1,128)S(1)}, f32[1,256]{1,0:T(1,128)}, u32[]{:S(2)}) copy-start(f32[1,256]{1,0:T(1,128)} %slice.834) | copy-start | bytes 3076
  225.7 6.9 %copy-start.26 = (f32[1,256]{1,0:T(1,128)S(1)}, f32[1,256]{1,0:T(1,128)}, u32[]{:S(2)}) copy-start(f32[1,256]{1,0:T(1,128)} %slice.808) | copy-start | bytes 3076
  232.6 1.6 copy-start.24
  234.1 1.8 copy-start.22
  235.9 0.7 copy-start.20
  236.0 0.7 slice-start
  236.7 41.9 %copy-start.5 = (f32[384,256]{1,0:T(8,128)}, f32[384,256]{1,0:T(8,128)S(1)}, u32[]{:S(2)}) copy-start(f32[384,256]{1,0:T(8,128)S(1)} %pad.226) | copy-start | bytes 1179652
  236.7 41.9 %copy-start.6 = (f32[384,256]{1,0:T(8,128)}, f32[384,256]{1,0:T(8,128)S(1)}, u32[]{:S(2)}) copy-start(f32[384,256]{1,0:T(8,128)S(1)} %pad.211) | copy-start | bytes 1179652
  283.7 33.9 %copy-start.9 = (bf16[64,256]{1,0:T(8,128)(2,1)S(1)}, bf16[64,256]{1,0:T(8,128)(2,1)}, u32[]{:S(2)}) copy-start(bf16[64,256]{1,0:T(8,128)(2,1)} %get-tuple-element.147) | copy-start | bytes 98308
  283.7 33.9 %copy-start.10 = (bf16[64,256]{1,0:T(8,128)(2,1)S(1)}, bf16[64,256]{1,0:T(8,128)(2,1)}, u32[]{:S(2)}) copy-start(bf16[64,256]{1,0:T(8,128)(2,1)} %get-tuple-element.218) | copy-start | bytes 98308
  283.7 54.4 %all-to-all-start.2 = ((bf16[8,384,256]{2,1,0:T(8,128)(2,1)}), bf16[8,384,256]{2,1,0:T(8,128)(2,1)S(1)}, u32[]{:S(2)}, u32[]{:S(2)}) async-start(bf16[8,384,256]{2,1,0:T(8,128)(2,1)} %bitcast.101), calls=%async_computation.2 | async-start | bytes 3145728 | tf_op jit(solution)/shard_map/all_to_all | solution.py:77
  317.5 20.8 %copy-start.2 = (bf16[384,256]{1,0:T(8,128)(2,1)S(1)}, bf16[384,256]{1,0:T(8,128)(2,1)}, u32[]{:S(2)}) copy-start(bf16[384,256]{1,0:T(8,128)(2,1)} %param.16) | copy-start | bytes 589828
  317.5 171.5 %all-gather.9.cloned.1.call-start = ((), (), s32[]{:S(2)}) async-start(), calls=%async_computation.8 | async-start | bytes 2162688 | tf_op jit(solution)/shard_map/all_gather | solution.py:30
  338.7 24.1 %copy-start.8 = (bf16[256,64]{0,1:T(8,128)(2,1)S(1)}, bf16[256,64]{0,1:T(8,128)(2,1)}, u32[]{:S(2)}) copy-start(bf16[256,64]{0,1:T(8,128)(2,1)} %get-tuple-element.152) | copy-start | bytes 98308
  363.9 206.9 %all-to-all-start.4 = ((bf16[32,256,64]{1,2,0:T(8,128)(2,1)}), bf16[32,256,64]{1,2,0:T(8,128)(2,1)}, u32[]{:S(2)}, u32[]{:S(2)}) async-start(bf16[32,256,64]{1,2,0:T(8,128)(2,1)} %stack.7), calls=%async_computation.4 | async-start | bytes 2097152 | tf_op jit(solution)/shard_map/all_to_all | solution.py:99
  380.5 115.1 %copy-start.16 = (f32[1,1,256]{2,1,0:T(1,128)S(1)}, f32[1,1,256]{2,1,0:T(1,128)}, u32[]{:S(2)}) copy-start(f32[1,1,256]{2,1,0:T(1,128)} %get-tuple-element.193) | copy-start | bytes 3076
  380.6 115.1 %copy-start.17 = (f32[1,1,256]{2,1,0:T(1,128)S(1)}, f32[1,1,256]{2,1,0:T(1,128)}, u32[]{:S(2)}) copy-start(f32[1,1,256]{2,1,0:T(1,128)} %get-tuple-element.194) | copy-start | bytes 3076
  380.6 115.1 %copy-start.18 = (f32[1,1,256]{2,1,0:T(1,128)S(1)}, f32[1,1,256]{2,1,0:T(1,128)}, u32[]{:S(2)}) copy-start(f32[1,1,256]{2,1,0:T(1,128)} %get-tuple-element.199) | copy-start | bytes 3076
  380.6 115.1 %copy-start.19 = (f32[1,1,256]{2,1,0:T(1,128)S(1)}, f32[1,1,256]{2,1,0:T(1,128)}, u32[]{:S(2)}) copy-start(f32[1,1,256]{2,1,0:T(1,128)} %get-tuple-element.200) | copy-start | bytes 3076
  380.6 115.3 %copy-start.34 = (f32[1,256]{1,0:T(1,128)S(1)}, f32[1,256]{1,0:T(1,128)}, u32[]{:S(2)}) copy-start(f32[1,256]{1,0:T(1,128)} %get-tuple-element.209) | copy-start | bytes 3076
  380.6 115.3 %copy-start.36 = (f32[384,256]{1,0:T(8,128)S(1)}, f32[384,256]{1,0:T(8,128)}, u32[]{:S(2)}) copy-start(f32[384,256]{1,0:T(8,128)} %param.24) | copy-start | bytes 1179652
  380.6 115.3 %copy-start.38 = (bf16[2,1,256,256]{3,2,1,0:T(8,128)(2,1)S(1)}, bf16[2,1,256,256]{3,2,1,0:T(8,128)(2,1)}, u32[]{:S(2)}) copy-start(bf16[2,1,256,256]{3,2,1,0:T(8,128)(2,1)} %param.20) | copy-start | bytes 786436
  380.6 115.3 %copy-start.41 = (f32[384]{0:T(512)S(1)}, f32[384]{0:T(512)}, u32[]{:S(2)}) copy-start(f32[384]{0:T(512)} %param.23) | copy-start | bytes 4612
  490.9 4.7 collective-permute-start.1
  497.5 18.7 %copy-start.1 = (f32[384,256]{1,0:T(8,128)}, f32[384,256]{1,0:T(8,128)S(1)}, u32[]{:S(2)}) copy-start(f32[384,256]{1,0:T(8,128)S(1)} %fusion.22) | copy-start | bytes 1179652
  514.5 8.2 %copy-start.31 = (f32[1,256]{1,0:T(1,128)S(1)}, f32[1,256]{1,0:T(1,128)}, u32[]{:S(2)}) copy-start(f32[1,256]{1,0:T(1,128)} %slice.868) | copy-start | bytes 3076
  514.5 8.3 %copy-start.11 = (f32[23,256]{1,0:T(8,128)S(1)}, f32[23,256]{1,0:T(8,128)}, u32[]{:S(2)}) copy-start(f32[23,256]{1,0:T(8,128)} %slice.737) | copy-start | bytes 70660
  514.5 8.3 %copy-start.12 = (f32[23,256]{1,0:T(8,128)S(1)}, f32[23,256]{1,0:T(8,128)}, u32[]{:S(2)}) copy-start(f32[23,256]{1,0:T(8,128)} %slice.772) | copy-start | bytes 70660
  514.5 8.3 %copy-start.29 = (f32[1,256]{1,0:T(1,128)S(1)}, f32[1,256]{1,0:T(1,128)}, u32[]{:S(2)}) copy-start(f32[1,256]{1,0:T(1,128)} %slice.893) | copy-start | bytes 3076
  514.5 8.4 %copy-start.27 = (f32[1,256]{1,0:T(1,128)S(1)}, f32[1,256]{1,0:T(1,128)}, u32[]{:S(2)}) copy-start(f32[1,256]{1,0:T(1,128)} %slice.867) | copy-start | bytes 3076
  514.5 8.4 %copy-start.7 = (f32[47,256]{1,0:T(8,128)S(1)}, f32[47,256]{1,0:T(8,128)}, u32[]{:S(2)}) copy-start(f32[47,256]{1,0:T(8,128)} %slice.774) | copy-start | bytes 144388
  522.8 2.4 copy-start.25
  525.1 1.8 copy-start.23
  526.9 0.7 copy-start.21
  527.0 0.7 slice-start.1
  527.7 43.1 %copy-start.3 = (f32[384,256]{1,0:T(8,128)}, f32[384,256]{1,0:T(8,128)S(1)}, u32[]{:S(2)}) copy-start(f32[384,256]{1,0:T(8,128)S(1)} %pad.258) | copy-start | bytes 1179652
  527.7 43.1 %copy-start.4 = (f32[384,256]{1,0:T(8,128)}, f32[384,256]{1,0:T(8,128)S(1)}, u32[]{:S(2)}) copy-start(f32[384,256]{1,0:T(8,128)S(1)} %pad.243) | copy-start | bytes 1179652
  628.7 8.5 %copy-start.33 = (f32[256]{0:T(256)S(1)}, f32[256]{0:T(256)}, u32[]{:S(2)}) copy-start(f32[256]{0:T(256)} %param.27) | copy-start | bytes 3076
Sparse Core Ops, SparseCore 0:
  9.4 200.5 all-gather.6
  320.4 168.5 all-gather.8
